TPU v7x, 32 devices: a whole 2x2x4 slice. The times are simulated.
32 devices in a mesh: grp: 2 (over y), sp: 4 (over z), tp: 4 (over x, core).
Axes of the slice: x: 2, y: 2, z: 4, core: 2. Of those that a mesh axis runs over, the one named last changes fastest.
Arguments:
- query_rows: bfloat16 [1024, 1024], P(('grp', 'sp'), 'tp'), parts along dimension 0, may hold values from -12 to 12
- key_rows: bfloat16 [1024, 1024], P(('grp', 'sp'), 'tp'), parts along dimension 0, may hold values from -9 to 9
- value_rows: bfloat16 [1024, 1024], P(('grp', 'sp'), 'tp'), parts along dimension 0, may hold values from -6 to 6
- key_logit: bfloat16 [1024, 8], P(('grp', 'sp'), 'tp'), parts along dimension 0, as said below
- residual: bfloat16 [1024, 2048], P(('grp', 'sp')), parts along dimension 0, may hold values from -6 to 6
- out_weight: bfloat16 [1024, 2048], P('tp'), may hold values from -0.1875 to 0.1875
- mix_gain: float32 [2048], replicated, may hold values from 0.1 to 1.9
- ffn_gain: float32 [2048], replicated, may hold values from 0.1 to 1.9
- out_gain: float32 [2048], replicated, may hold values from 0.1 to 1.9
- gate_weight: bfloat16 [2048, 5120], P('sp', 'tp'), may hold values from -0.125 to 0.125
- up_weight: bfloat16 [2048, 5120], P('sp', 'tp'), may hold values from -0.125 to 0.125
- down_weight: bfloat16 [2048, 5120], P('sp', 'tp'), may hold values from -0.078125 to 0.078125
Outputs:
- layer_out: bfloat16 [1024, 2048], P(('grp', 'sp')), parts along dimension 0
There are 2 independent parts, one for each index of `grp`. A program takes and returns all parts, laid end to end along the dimension named above; an argument that names none is the same for every part. Nothing has to cross between parts.
Inputs may be any that keep to these rules, and one draw needn't show every extreme that they name: `key_logit`: log-odds offsets of the keys, all negative.
All inputs are finite; a program needn't handle non-finite values.
Results may differ from a plain program's by a relative error of at most 0.018.
Values may be sent and summed in bfloat16 or wider, within the bound.
No kernel may reach another device: no remote copies, remote signals or barrier semaphores. Data moves between devices by JAX's collectives and lax.ppermute only.
A program may use at most 64 MiB of HBM per device.

v0:
```python
import jax
import jax.numpy as jnp
from jax import lax
from jax.sharding import PartitionSpec as P

epsilon = 1e-06


def normalize(payload_table):
    return payload_table * lax.rsqrt(
        jnp.mean(payload_table * payload_table, axis=-1, keepdims=True) + epsilon
    )


def shards(
    query_rows,
    key_rows,
    value_rows,
    key_logit,
    residual,
    out_weight,
    mix_gain,
    ffn_gain,
    out_gain,
    gate_weight,
    up_weight,
    down_weight,
):
    tok_rows = query_rows.shape[0]
    head_count = key_logit.shape[1]
    head_width = query_rows.shape[1] // head_count
    block_count = lax.axis_size("sp")
    own_block = lax.axis_index("sp")
    queries = query_rows.reshape(tok_rows, head_count, head_width).transpose(1, 0, 2)
    score_scale = head_width ** (-0.5)
    query_pos = own_block * tok_rows + jnp.arange(tok_rows, dtype=jnp.int32)[:, None]

    def group_terms(key_part, value_part, logit_part, first_block):
        span_rows = key_part.shape[0]
        shard_count = span_rows // tok_rows

        def compute(unused):
            scores = (
                jnp.einsum(
                    "hqd,khd->hqk",
                    queries,
                    key_part.reshape(span_rows, head_count, head_width),
                    preferred_element_type=jnp.float32,
                )
                * score_scale
            )
            scores = scores + jnp.transpose(logit_part.astype(jnp.float32))[:, None, :]
            key_pos = first_block * tok_rows + jnp.arange(span_rows, dtype=jnp.int32)[None, :]
            causal = (key_pos < query_pos).reshape(tok_rows, shard_count, tok_rows)
            scores = scores.reshape(head_count, tok_rows, shard_count, tok_rows)
            keep_log = jnp.where(causal, jax.nn.log_sigmoid(-scores), 0.0)
            within = lax.cumsum(keep_log, axis=3, reverse=True) - keep_log
            sticks = jnp.where(causal, jnp.exp(jax.nn.log_sigmoid(scores) + within), 0.0).astype(
                jnp.bfloat16
            )
            partials = jnp.einsum(
                "hqgk,gkhd->ghqd",
                sticks,
                value_part.reshape(shard_count, tok_rows, head_count, head_width),
                preferred_element_type=jnp.float32,
            )
            return (jnp.sum(keep_log, axis=3), partials)

        def skipped(unused):
            return (
                jnp.zeros((head_count, tok_rows, shard_count), jnp.float32),
                jnp.zeros((shard_count, head_count, tok_rows, head_width), jnp.float32),
            )

        return lax.cond(first_block <= own_block, compute, skipped, 0)

    initial = (
        jnp.zeros((head_count, tok_rows, block_count), jnp.float32),
        jnp.zeros((block_count, head_count, tok_rows, head_width), jnp.float32),
    )
    tables = initial
    key_part = lax.all_gather(key_rows, "sp", axis=0, tiled=True)
    value_part = lax.all_gather(value_rows, "sp", axis=0, tiled=True)
    logit_part = lax.all_gather(key_logit, "sp", axis=0, tiled=True)
    shard_count = key_part.shape[0] // tok_rows
    group_size = 2
    span_rows = group_size * tok_rows

    def one_group(carried, group_index):
        offset = group_index * span_rows
        first_block = group_index * group_size
        totals, partials = group_terms(
            lax.dynamic_slice_in_dim(key_part, offset, span_rows, 0),
            lax.dynamic_slice_in_dim(value_part, offset, span_rows, 0),
            lax.dynamic_slice_in_dim(logit_part, offset, span_rows, 0),
            first_block,
        )
        carried = (
            lax.dynamic_update_slice(carried[0], totals, (0, 0, first_block)),
            lax.dynamic_update_slice(carried[1], partials, (first_block, 0, 0, 0)),
        )
        return (carried, None)

    tables, unused = lax.scan(
        one_group, tables, jnp.arange(shard_count // group_size, dtype=jnp.int32)
    )
    totals, partials = tables
    suffix = lax.cumsum(totals, axis=2, reverse=True) - totals
    attended = jnp.einsum(
        "hqb,bhqd->qhd", jnp.exp(suffix), partials, precision=lax.Precision.HIGHEST
    )
    attended = attended.reshape(tok_rows, head_count * head_width).astype(jnp.bfloat16)
    head_part = jnp.dot(attended, out_weight, preferred_element_type=jnp.float32)
    mixed_rows = lax.psum(head_part.astype(jnp.bfloat16), "tp")
    middle = (
        residual.astype(jnp.float32) + mix_gain * normalize(mixed_rows.astype(jnp.float32))
    ).astype(jnp.bfloat16)
    normed = (ffn_gain * normalize(middle.astype(jnp.float32))).astype(jnp.bfloat16)
    gate_act = jnp.dot(
        normed,
        lax.all_gather(gate_weight, "sp", axis=0, tiled=True),
        preferred_element_type=jnp.float32,
    )
    up_act = jnp.dot(
        normed,
        lax.all_gather(up_weight, "sp", axis=0, tiled=True),
        preferred_element_type=jnp.float32,
    )
    hidden = (jax.nn.silu(gate_act) * up_act).astype(jnp.bfloat16)
    unit_part = lax.dot_general(
        hidden,
        lax.all_gather(down_weight, "sp", axis=0, tiled=True),
        (((1,), (1,)), ((), ())),
        preferred_element_type=jnp.float32,
    )
    ffn_out = lax.psum(unit_part.astype(jnp.bfloat16), "tp")
    return (middle.astype(jnp.float32) + out_gain * normalize(ffn_out.astype(jnp.float32))).astype(
        jnp.bfloat16
    )


def solution(mesh):
    placed = (
        P(("grp", "sp"), "tp"),
        P(("grp", "sp"), "tp"),
        P(("grp", "sp"), "tp"),
        P(("grp", "sp"), "tp"),
        P(("grp", "sp"), None),
        P("tp", None),
        P(),
        P(),
        P(),
        P("sp", "tp"),
        P("sp", "tp"),
        P("sp", "tp"),
    )
    return jax.shard_map(
        shards, mesh=mesh, in_specs=placed, out_specs=P(("grp", "sp"), None), check_vma=False
    )
```

profile of v0, /device:TPU:0, one launch (start us, length us, event | category | flops | bytes accessed | tf_op | source)
XLA Modules:
  0.0 408.5 jit_solution(9131922966451456633)
XLA Ops:
  7.4 1.0 copy.41
  8.4 14.5 %all_gather.18 = bf16[512,256]{0,1:T(8,128)(2,1)S(1)} all-gather(bf16[128,256]{0,1:T(8,128)(2,1)S(1)} %copy.41), channel_id=1, replica_groups=mesh['grp'=2,'sp'=4,'tp'=4] {'sp'}, dimensions={0}, use_global_device_ids=true | all-gather | bytes 327680 | tf_op jit(solution)/shard_map/all_gather | solution.py:82
  22.9 14.6 %all_gather.20 = bf16[512,256]{1,0:T(8,128)(2,1)S(1)} all-gather(bf16[128,256]{1,0:T(8,128)(2,1)} %param.18), channel_id=1, replica_groups=mesh['grp'=2,'sp'=4,'tp'=4] {'sp'}, dimensions={0}, use_global_device_ids=true | all-gather | bytes 327680 | tf_op jit(solution)/shard_map/all_gather | solution.py:83
  37.5 0.9 copy.42
  38.6 10.0 %all_gather.19 = bf16[512,2]{0,1:T(2,128)(2,1)S(1)} all-gather(bf16[128,2]{0,1:T(2,128)(2,1)} %param.19), channel_id=1, replica_groups=mesh['grp'=2,'sp'=4,'tp'=4] {'sp'}, dimensions={0}, use_global_device_ids=true | all-gather | bytes 2560 | tf_op jit(solution)/shard_map/all_gather | solution.py:84
  48.7 8.5 %while.13 = (s32[]{:T(128)}, f32[2,128,4]{1,2,0:T(4,128)S(1)}, f32[4,2,128,128]{3,0,1,2:T(4,128)S(1)}, s32[2]{0:T(128)S(1)}, s32[]{:T(128)}, /*index=5*/bf16[512...) while((s32[]{:T(128)}, f32[2,128,4]{1,2,0:T(4,128)S(1)}, ...), condition=%wide.region_5.6_spmd.clone, body=%wide.region_0.5_spmd.clone.sunk | while | flops 43418504 | bytes 4373875 | solution.py:104
  48.7 0.6 dynamic_slice.39
  49.9 5.3 %conditional.3 = (f32[2,128,2]{1,2,0:T(2,128)S(1)}, f32[2,2,128,128]{3,2,1,0:T(8,128)S(1)}) conditional(s32[]{:T(128)} %convert_element_type.116, () %tuple.48, (s32[]{:T(128)}, s32[]{:T(128)}, s32[]{:T(128)}, bf16[512,256]{0,1:T(8,128)(2,1)S(1)}, bf16[2,128,128]{2,1,0:T(8,128)(2,1)S(1)}, /*index=5*/bf16[512,2]{0,1:T(2,128)(2,1)S(1)}, ...), branch_computations={%region_1.1_spmd, %region_2.4_spmd} | conditional | flops 43418500 | bytes 3844702 | solution.py:75
  50.6 0.2 fusion.2
  51.1 0.8 fusion.35
  51.9 2.2 fusion.38
  54.0 0.9 select_convert_fusion
  55.0 0.2 fusion.8
  55.2 0.3 copy_dynamic-update-slice_fusion.2
  55.6 0.6 dynamic_slice.39
  56.9 0.3 copy_dynamic-update-slice_fusion.2
  57.5 1.8 fusion.39
  59.3 1.1 convolution_convert_fusion.1
  60.5 0.5 all-gather.4.cloned.1.call-update
  61.1 0.5 all-gather.6.cloned.1.call-update
  61.7 0.5 all-gather.8.cloned.1.call-update
  62.2 34.5 %all-reduce.3.cloned.1.call-done = bf16[128,2048]{1,0:T(8,128)(2,1)} async-done(((bf16[128,2048]{1,0:T(8,128)(2,1)}), bf16[128,2048]{1,0:T(8,128)(2,1)}) %all-reduce.3.cloned.1.call-update) | async-done | bytes 524304 | tf_op jit(solution)/shard_map/psum | solution.py:114
  96.8 1.2 fusion.12
  98.0 1.5 fusion.18
  99.5 63.6 %all-gather.4.cloned.1.call-done = bf16[2048,1280]{1,0:T(8,128)(2,1)} async-done(((bf16[512,1280]{1,0:T(8,128)(2,1)}), bf16[2048,1280]{1,0:T(8,128)(2,1)}) %all-gather.4.cloned.1.call-update) | async-done | bytes 5242896 | tf_op jit(solution)/shard_map/all_gather | solution.py:121
  163.1 3.4 fusion.30
  166.5 94.3 %all-gather.6.cloned.1.call-done = bf16[2048,1280]{1,0:T(8,128)(2,1)} async-done(((bf16[512,1280]{1,0:T(8,128)(2,1)}), bf16[2048,1280]{1,0:T(8,128)(2,1)}) %all-gather.6.cloned.1.call-update) | async-done | bytes 5242896 | tf_op jit(solution)/shard_map/all_gather | solution.py:126
  260.8 97.7 %all-gather.8.cloned.1.call-done = bf16[2048,1280]{1,0:T(8,128)(2,1)} async-done(((bf16[512,1280]{1,0:T(8,128)(2,1)}), bf16[2048,1280]{1,0:T(8,128)(2,1)}) %all-gather.8.cloned.1.call-update) | async-done | bytes 5242896 | tf_op jit(solution)/shard_map/all_gather | solution.py:132
  358.5 7.2 %convolution_convert_fusion = bf16[128,2048]{1,0:T(8,128)(2,1)} fusion(bf16[2048,1280]{1,0:T(8,128)(2,1)} %all-gather.8.cloned.1.call-done, bf16[2048,1280]{1,0:T(8,128)(2,1)} %all-gather.6.cloned.1.call-done, f32[128,1280]{1,0:T(8,128)S(1)} %fusion.30, bf16[128,2048]{1,0:T(8,128)(2,1)S(1)} %get-tuple-element.241, f32[128]{0:T(128)S(1)} %add_rsqrt_fusion.1, ...), kind=kOutput, calls=%fused_computation.23 | convolution fusion | flops 1344471040 | bytes 12198400 | tf_op jit(solution)/shard_map/dot_general | solution.py:130
  365.7 31.9 %all-reduce.5.cloned.1.call-done = bf16[128,2048]{1,0:T(8,128)(2,1)} async-done(((bf16[128,2048]{1,0:T(8,128)(2,1)}), bf16[128,2048]{1,0:T(8,128)(2,1)}) %all-reduce.5.cloned.1.call-update) | async-done | bytes 524304 | tf_op jit(solution)/shard_map/psum | solution.py:136
  397.6 1.2 fusion.16
  398.9 2.1 fusion.21
  (42 shorter events, 1.1 us)
Async XLA Ops:
  7.4 51.9 %copy-start = (bf16[256,2048]{1,0:T(8,128)(2,1)S(1)}, bf16[256,2048]{1,0:T(8,128)(2,1)}, u32[]{:S(2)}) copy-start(bf16[256,2048]{1,0:T(8,128)(2,1)} %param.21) | copy-start | bytes 3145732
  7.4 89.4 %all-reduce.3.cloned.1.call-start = ((), (), s32[]{:S(2)}) async-start(), calls=%async_computation | async-start | bytes 1048576 | tf_op jit(solution)/shard_map/psum | solution.py:114
  57.2 40.8 %copy-start.1 = (bf16[128,2048]{1,0:T(8,128)(2,1)S(1)}, bf16[128,2048]{1,0:T(8,128)(2,1)}, u32[]{:S(2)}) copy-start(bf16[128,2048]{1,0:T(8,128)(2,1)} %param.20) | copy-start | bytes 1572868
  57.2 40.8 %copy-start.2 = (f32[2048]{0:T(1024)S(1)}, f32[2048]{0:T(1024)}, u32[]{:S(2)}) copy-start(f32[2048]{0:T(1024)} %param.22) | copy-start | bytes 24580
  57.2 105.8 %copy-start.3 = (f32[2048]{0:T(1024)S(1)}, f32[2048]{0:T(1024)}, u32[]{:S(2)}) copy-start(f32[2048]{0:T(1024)} %param.23) | copy-start | bytes 24580
  60.4 102.6 %all-gather.4.cloned.1.call-start = ((), (), s32[]{:S(2)}) async-start(), calls=%async_computation.1 | async-start | bytes 6553600 | tf_op jit(solution)/shard_map/all_gather | solution.py:121
  61.0 199.8 %all-gather.6.cloned.1.call-start = ((), (), s32[]{:S(2)}) async-start(), calls=%async_computation.2 | async-start | bytes 6553600 | tf_op jit(solution)/shard_map/all_gather | solution.py:126
  61.6 296.9 %all-gather.8.cloned.1.call-start = ((), (), s32[]{:S(2)}) async-start(), calls=%async_computation.3 | async-start | bytes 6553600 | tf_op jit(solution)/shard_map/all_gather | solution.py:132
  62.2 335.4 %all-reduce.5.cloned.1.call-start = ((), (), s32[]{:S(2)}) async-start(), calls=%async_computation.4 | async-start | bytes 1048576 | tf_op jit(solution)/shard_map/psum | solution.py:136
  166.5 232.4 %copy-start.4 = (f32[2048]{0:T(1024)S(1)}, f32[2048]{0:T(1024)}, u32[]{:S(2)}) copy-start(f32[2048]{0:T(1024)} %param.24) | copy-start | bytes 24580
Sparse Core Ops, SparseCore 0:
  60.6 36.1 all-reduce.2
  365.9 31.7 all-reduce.4
Sparse Core Ops, SparseCore 1:
  62.5 100.5 all-gather.3
  164.5 96.2 all-gather.5
  262.2 96.2 all-gather.7
where the time goes:
time: 409 us
  waiting for transfers between devices  324 us (79%)
  blocking collectives  39.1 us (10%)
  between operations  15.1 us (4%)
  matrix products  14 us (3%)
  other arithmetic  10.2 us (2%)
  local copies, waits for them, and re-layouts  4.28 us (1%)
    all_gather x1, waiting for transfers between devices, shards(): lax.all_gather(down_weight, 'sp', axis=0, tiled=True)  97.7 us
    all_gather x1, waiting for transfers between devices, shards(): lax.all_gather(up_weight, 'sp', axis=0, tiled=True)  94.3 us
    all_gather x1, waiting for transfers between devices, shards(): lax.all_gather(gate_weight, 'sp', axis=0, tiled=True)  63.6 us
    psum x1, waiting for transfers between devices, shards(): mixed_rows = lax.psum(head_part.astype(jnp.bfloat16), 'tp')  34.5 us
    psum x1, waiting for transfers between devices, shards(): ffn_out = lax.psum(unit_part.astype(jnp.bfloat16), 'tp')  31.9 us
    all_gather x1, blocking collectives, shards(): value_part = lax.all_gather(value_rows, 'sp', axis=0, tiled=True)  14.6 us
    all_gather x1, blocking collectives, shards(): key_part = lax.all_gather(key_rows, 'sp', axis=0, tiled=True)  14.5 us
    all_gather x1, blocking collectives, shards(): logit_part = lax.all_gather(key_logit, 'sp', axis=0, tiled=True)  10 us
  transfers between devices with their start and end apart: 5, of which 5 were waited for; matrix products, arithmetic and copies ran while one was open for 1% of the time, Pallas kernels for 0%

commit v1 on v0

--- a/solution.py
+++ b/solution.py
@@ -80,8 +80,12 @@
     )
     tables = initial
     key_part = lax.all_gather(key_rows, "sp", axis=0, tiled=True)
-    value_part = lax.all_gather(value_rows, "sp", axis=0, tiled=True)
-    logit_part = lax.all_gather(key_logit, "sp", axis=0, tiled=True)
+    press_lane = lambda array_here, u: jnp.split(
+        jax.lax.all_gather(jnp.concatenate([array_here, u], axis=1), "sp", axis=0, tiled=True),
+        [array_here.shape[1]],
+        axis=1,
+    )
+    value_part, logit_part = press_lane(value_rows, key_logit)
     shard_count = key_part.shape[0] // tok_rows
     group_size = 2
     span_rows = group_size * tok_rows

time: 409 us -> 405 us (level)
  blocking collectives: 39.1 us -> 29.6 us
    all_gather x2 -> x1, blocking collectives: 24.6 us -> 16.3 us  [shards(): jax.lax.all_gather(jnp.concatenate([array_here, u], axis=1), 'sp', axis=0...]
  transfers between devices with their start and end apart: 5 -> 5, of which waited for: 5 -> 5; matrix products, arithmetic and copies ran while one was open for 1% -> 2% of each run, Pallas kernels for 0% -> 0%
where the time goes in v1:
time: 405 us; the launch traced here: 404 us
  waiting for transfers between devices  327 us (81%)
  blocking collectives  29.6 us (7%)
  between operations  15.2 us (4%)
  matrix products  14 us (3%)
  other arithmetic  11 us (3%)
  local copies, waits for them, and re-layouts  5.22 us (1%)
    all_gather x1, waiting for transfers between devices, shards(): lax.all_gather(down_weight, 'sp', axis=0, tiled=True)  97.7 us
    all_gather x1, waiting for transfers between devices, shards(): lax.all_gather(up_weight, 'sp', axis=0, tiled=True)  94.3 us
    all_gather x1, waiting for transfers between devices, shards(): lax.all_gather(gate_weight, 'sp', axis=0, tiled=True)  63.6 us
    psum x1, waiting for transfers between devices, shards(): mixed_rows = lax.psum(head_part.astype(jnp.bfloat16), 'tp')  37.6 us
    psum x1, waiting for transfers between devices, shards(): ffn_out = lax.psum(unit_part.astype(jnp.bfloat16), 'tp')  31.9 us
    all_gather x1, blocking collectives, shards(): jax.lax.all_gather(jnp.concatenate([array_here, u], axis=1), 'sp', axis=0...  16.3 us
    all_gather x1, blocking collectives, shards(): key_part = lax.all_gather(key_rows, 'sp', axis=0, tiled=True)  13.4 us
  transfers between devices with their start and end apart: 5, of which 5 were waited for; matrix products, arithmetic and copies ran while one was open for 2% of the time, Pallas kernels for 0%

profile of v1, /device:TPU:0, one launch (start us, length us, event | category | flops | bytes accessed | tf_op | source)
XLA Modules:
  0.0 404.0 jit_solution(16098828212318033610)
XLA Ops:
  7.4 0.9 copy.47
  8.2 0.9 pad_maximum_fusion
  9.1 16.3 %all_gather.16 = bf16[512,258]{1,0:T(8,128)(2,1)S(1)} all-gather(bf16[128,258]{1,0:T(8,128)(2,1)S(1)} %pad_maximum_fusion), channel_id=1, replica_groups=mesh['grp'=2,'sp'=4,'tp'=4] {'sp'}, dimensions={0}, use_global_device_ids=true | all-gather | bytes 330240 | tf_op jit(solution)/shard_map/all_gather | solution.py:84
  25.5 1.0 copy.45
  26.5 13.4 %all_gather.15 = bf16[512,256]{0,1:T(8,128)(2,1)S(1)} all-gather(bf16[128,256]{0,1:T(8,128)(2,1)S(1)} %copy.45), channel_id=1, replica_groups=mesh['grp'=2,'sp'=4,'tp'=4] {'sp'}, dimensions={0}, use_global_device_ids=true | all-gather | bytes 327680 | tf_op jit(solution)/shard_map/all_gather | solution.py:82
  39.9 0.9 copy.46
  41.0 8.5 %while.13 = (s32[]{:T(128)}, f32[2,128,4]{1,2,0:T(4,128)S(1)}, f32[4,2,128,128]{3,0,1,2:T(4,128)S(1)}, s32[2]{0:T(128)S(1)}, s32[]{:T(128)}, /*index=5*/bf16[512...) while((s32[]{:T(128)}, f32[2,128,4]{1,2,0:T(4,128)S(1)}, ...), condition=%wide.region_5.6_spmd.clone, body=%wide.region_0.5_spmd.clone.sunk | while | flops 43418504 | bytes 4373875 | solution.py:108
  41.1 0.6 dynamic_slice.39
  42.3 5.3 %conditional.3 = (f32[2,128,2]{1,2,0:T(2,128)S(1)}, f32[2,2,128,128]{3,2,1,0:T(8,128)S(1)}) conditional(s32[]{:T(128)} %convert_element_type.116, () %tuple.49, (s32[]{:T(128)}, s32[]{:T(128)}, s32[]{:T(128)}, bf16[512,256]{0,1:T(8,128)(2,1)S(1)}, bf16[2,128,128]{2,1,0:T(8,128)(2,1)S(1)}, /*index=5*/bf16[512,2]{0,1:T(2,128)(2,1)S(1)}, ...), branch_computations={%region_1.1_spmd, %region_2.4_spmd} | conditional | flops 43418500 | bytes 3844702 | solution.py:75
  43.0 0.2 fusion.2
  43.5 0.8 fusion.35
  44.2 2.2 fusion.38
  46.4 0.9 select_convert_fusion
  47.6 0.3 copy_dynamic-update-slice_fusion.2
  48.0 0.6 dynamic_slice.39
  49.3 0.3 copy_dynamic-update-slice_fusion.2
  49.8 1.8 fusion.39
  51.7 1.1 convolution_convert_fusion.1
  52.9 0.5 all-gather.4.cloned.1.call-update
  53.5 0.5 all-gather.6.cloned.1.call-update
  54.1 0.5 all-gather.8.cloned.1.call-update
  54.6 37.6 %all-reduce.3.cloned.1.call-done = bf16[128,2048]{1,0:T(8,128)(2,1)} async-done(((bf16[128,2048]{1,0:T(8,128)(2,1)}), bf16[128,2048]{1,0:T(8,128)(2,1)}) %all-reduce.3.cloned.1.call-update) | async-done | bytes 524304 | tf_op jit(solution)/shard_map/psum | solution.py:118
  92.3 1.2 fusion.12
  93.5 1.5 fusion.18
  95.0 63.6 %all-gather.4.cloned.1.call-done = bf16[2048,1280]{1,0:T(8,128)(2,1)} async-done(((bf16[512,1280]{1,0:T(8,128)(2,1)}), bf16[2048,1280]{1,0:T(8,128)(2,1)}) %all-gather.4.cloned.1.call-update) | async-done | bytes 5242896 | tf_op jit(solution)/shard_map/all_gather | solution.py:125
  158.6 3.4 fusion.30
  162.0 94.3 %all-gather.6.cloned.1.call-done = bf16[2048,1280]{1,0:T(8,128)(2,1)} async-done(((bf16[512,1280]{1,0:T(8,128)(2,1)}), bf16[2048,1280]{1,0:T(8,128)(2,1)}) %all-gather.6.cloned.1.call-update) | async-done | bytes 5242896 | tf_op jit(solution)/shard_map/all_gather | solution.py:130
  256.3 97.7 %all-gather.8.cloned.1.call-done = bf16[2048,1280]{1,0:T(8,128)(2,1)} async-done(((bf16[512,1280]{1,0:T(8,128)(2,1)}), bf16[2048,1280]{1,0:T(8,128)(2,1)}) %all-gather.8.cloned.1.call-update) | async-done | bytes 5242896 | tf_op jit(solution)/shard_map/all_gather | solution.py:136
  354.0 7.2 %convolution_convert_fusion = bf16[128,2048]{1,0:T(8,128)(2,1)} fusion(bf16[2048,1280]{1,0:T(8,128)(2,1)} %all-gather.8.cloned.1.call-done, bf16[2048,1280]{1,0:T(8,128)(2,1)} %all-gather.6.cloned.1.call-done, f32[128,1280]{1,0:T(8,128)S(1)} %fusion.30, bf16[128,2048]{1,0:T(8,128)(2,1)S(1)} %get-tuple-element.251, f32[128]{0:T(128)S(1)} %add_rsqrt_fusion.1, ...), kind=kOutput, calls=%fused_computation.23 | convolution fusion | flops 1344471040 | bytes 12198400 | tf_op jit(solution)/shard_map/dot_general | solution.py:134
  361.2 31.9 %all-reduce.5.cloned.1.call-done = bf16[128,2048]{1,0:T(8,128)(2,1)} async-done(((bf16[128,2048]{1,0:T(8,128)(2,1)}), bf16[128,2048]{1,0:T(8,128)(2,1)}) %all-reduce.5.cloned.1.call-update) | async-done | bytes 524304 | tf_op jit(solution)/shard_map/psum | solution.py:140
  393.1 1.2 fusion.16
  394.4 2.1 fusion.21
  (46 shorter events, 1.5 us)
Async XLA Ops:
  7.4 44.3 %copy-start = (bf16[256,2048]{1,0:T(8,128)(2,1)S(1)}, bf16[256,2048]{1,0:T(8,128)(2,1)}, u32[]{:S(2)}) copy-start(bf16[256,2048]{1,0:T(8,128)(2,1)} %param.21) | copy-start | bytes 3145732
  7.4 84.9 %all-reduce.3.cloned.1.call-start = ((), (), s32[]{:S(2)}) async-start(), calls=%async_computation | async-start | bytes 1048576 | tf_op jit(solution)/shard_map/psum | solution.py:118
  49.6 43.9 %copy-start.1 = (bf16[128,2048]{1,0:T(8,128)(2,1)S(1)}, bf16[128,2048]{1,0:T(8,128)(2,1)}, u32[]{:S(2)}) copy-start(bf16[128,2048]{1,0:T(8,128)(2,1)} %param.20) | copy-start | bytes 1572868
  49.6 43.9 %copy-start.2 = (f32[2048]{0:T(1024)S(1)}, f32[2048]{0:T(1024)}, u32[]{:S(2)}) copy-start(f32[2048]{0:T(1024)} %param.22) | copy-start | bytes 24580
  49.6 109.0 %copy-start.3 = (f32[2048]{0:T(1024)S(1)}, f32[2048]{0:T(1024)}, u32[]{:S(2)}) copy-start(f32[2048]{0:T(1024)} %param.23) | copy-start | bytes 24580
  52.9 105.7 %all-gather.4.cloned.1.call-start = ((), (), s32[]{:S(2)}) async-start(), calls=%async_computation.1 | async-start | bytes 6553600 | tf_op jit(solution)/shard_map/all_gather | solution.py:125
  53.4 202.8 %all-gather.6.cloned.1.call-start = ((), (), s32[]{:S(2)}) async-start(), calls=%async_computation.2 | async-start | bytes 6553600 | tf_op jit(solution)/shard_map/all_gather | solution.py:130
  54.0 300.0 %all-gather.8.cloned.1.call-start = ((), (), s32[]{:S(2)}) async-start(), calls=%async_computation.3 | async-start | bytes 6553600 | tf_op jit(solution)/shard_map/all_gather | solution.py:136
  54.6 338.5 %all-reduce.5.cloned.1.call-start = ((), (), s32[]{:S(2)}) async-start(), calls=%async_computation.4 | async-start | bytes 1048576 | tf_op jit(solution)/shard_map/psum | solution.py:140
  162.0 232.4 %copy-start.4 = (f32[2048]{0:T(1024)S(1)}, f32[2048]{0:T(1024)}, u32[]{:S(2)}) copy-start(f32[2048]{0:T(1024)} %param.24) | copy-start | bytes 24580
Sparse Core Ops, SparseCore 0:
  53.0 39.2 all-reduce.2
  361.4 31.7 all-reduce.4
Sparse Core Ops, SparseCore 1:
  54.9 103.6 all-gather.3
  160.0 96.2 all-gather.5
  257.7 96.2 all-gather.7
